TPU v7x, 32 devices: a whole 2x2x4 slice. The times are simulated.
32 devices in a mesh: grp: 2 (over y), sp: 4 (over z), tp: 4 (over x, core).
Axes of the slice: x: 2, y: 2, z: 4, core: 2. Of those that a mesh axis runs over, the one named last changes fastest.
Arguments:
- query_rows: bfloat16 [3072, 2048], P(('grp', 'sp'), 'tp'), parts along dimension 0, may hold values from -6 to 6, as said below
- key_rows: bfloat16 [3072, 1024], P(('grp', 'sp'), 'tp'), parts along dimension 0, may hold values from -6 to 6, as said below
- value_rows: bfloat16 [3072, 1024], P(('grp', 'sp'), 'tp'), parts along dimension 0, may hold values from -15 to 15
- pool_input: bfloat16 [3072, 2048], P(('grp', 'sp'), 'tp'), parts along dimension 0, may hold values from -6 to 6
- log_gate_sums: float32 [3072, 16], P(('grp', 'sp'), 'tp'), parts along dimension 0, as said below
- query_gain: float32 [128], replicated, may hold values from 0.7 to 4.5, as said below
- key_gain: float32 [128], replicated, may hold values from 0.7 to 4.5, as said below
- pool_weight: bfloat16 [8, 256, 256], P('tp'), may hold values from -0.375 to 0.375
- pool_scale: float32 [2048], P('tp'), may hold values from 0.1 to 1.9
- attention_out: bfloat16 [2048, 4096], P('tp'), may hold values from -0.09375 to 0.09375
- pooling_out: bfloat16 [2048, 4096], P('tp'), may hold values from -0.09375 to 0.09375
Outputs:
- mixed_rows: bfloat16 [3072, 4096], P(('grp', 'sp', 'tp')), parts along dimension 0
There are 2 independent parts, one for each index of `grp`. A program takes and returns all parts, laid end to end along the dimension named above; an argument that names none is the same for every part. Nothing has to cross between parts.
Inputs may be any that keep to these rules, and one draw needn't show every extreme that they name: `query_rows`: normal entries; in some rows a query head's entries may equal its key head's entries of an earlier position. `key_rows`: normal entries. `log_gate_sums`: each column never rises from one position to the next. `query_gain`: Positive. `key_gain`: Positive.
All inputs are finite; a program needn't handle non-finite values.
Results may differ from a plain program's by a relative error of at most 0.014.
The roundings to bfloat16 on the way count: a program that leaves them out, or rounds other values in their place, can miss the bound.
Values may be sent and summed in bfloat16 or wider, within the bound.
A program may use at most 64 MiB of HBM per device.

v0:
```python
import math
import jax
import jax.numpy as jnp
from jax import lax
from jax.sharding import PartitionSpec as P

HEAD = 128
QUERY_HEADS = 16
KV_HEADS = 8
GROUP = 256
MAX_WINDOW = 16
epsilon = 1e-06
masked = -1e30


def from_behind(block, axis, distance):
    devices = range(lax.axis_size(axis))
    route = [(i - distance, i) for i in devices if i - distance in devices]
    return lax.ppermute(block, axis, route)


def head_norm(row_data, gain_vector, head_count):
    shaped = row_data.astype(jnp.float32).reshape(row_data.shape[0], head_count, -1)
    scaled = shaped * lax.rsqrt(jnp.mean(shaped * shaped, axis=-1, keepdims=True) + epsilon)
    return (scaled * gain_vector).astype(jnp.bfloat16)


def window_means(padded, length, first_pos, windows):
    rim_rows = padded.shape[0] - length
    window_sum = jnp.zeros((length,) + padded.shape[1:], jnp.float32)
    pooled = window_sum
    for lookback in range(rim_rows + 1):
        window_sum = window_sum + padded[rim_rows - lookback : rim_rows - lookback + length]
        window_size = lookback + 1
        if window_size >= 2 and window_size & window_size - 1 == 0:
            pooled = jnp.where((windows == window_size)[None, :, None], window_sum, pooled)
    positions = (first_pos + jnp.arange(length, dtype=jnp.int32)).astype(jnp.float32)
    counts = jnp.minimum(positions[:, None, None] + 1.0, windows.astype(jnp.float32)[None, :, None])
    return pooled / counts - padded[rim_rows:]


def attend_block(running, queries, query_gates, query_pos, pair_block, key_gates, key_pos):
    row_best, weight_sum, accumulated = running
    scores = jnp.einsum(
        "tkrd,skd->krts", queries, pair_block[0], preferred_element_type=jnp.float32
    )
    scores = scores * (1.0 / math.sqrt(HEAD)) + query_gates - key_gates
    allowed = key_pos[None, :] <= query_pos[:, None]
    scores = jnp.where(allowed, scores, masked)
    new_best = jnp.maximum(row_best, jnp.max(scores, axis=-1, keepdims=True))
    weights = jnp.where(allowed, jnp.exp(scores - new_best), 0.0)
    fading = jnp.exp(row_best - new_best)
    weight_sum = weight_sum * fading + jnp.sum(weights, axis=-1, keepdims=True)
    summed = jnp.einsum(
        "krts,skd->krtd",
        weights.astype(jnp.bfloat16),
        pair_block[1],
        preferred_element_type=jnp.float32,
    )
    return (new_best, weight_sum, accumulated * fading + summed)


def attend_piece(running, piece, queries, query_gates, query_pos, all_gates, valid):
    kv_here = queries.shape[1]
    ratio = queries.shape[2]
    piece_rows = piece.shape[1]
    block_rows = piece_rows
    while block_rows > 1024 and block_rows % 2 == 0:
        block_rows = block_rows // 2
    last_query = query_pos[query_pos.shape[0] - 1]

    def one_block(block_index, loop_state):
        first = block_index * block_rows

        def compute(state):
            pair_block = lax.dynamic_slice_in_dim(piece, block_index * block_rows, block_rows, 1)
            gate_block = lax.dynamic_slice_in_dim(all_gates, jnp.maximum(first, 0), block_rows, 0)
            gate_block = gate_block.T.reshape(kv_here, ratio, 1, block_rows)
            key_pos = first + jnp.arange(block_rows, dtype=jnp.int32)
            return attend_block(
                state, queries, query_gates, query_pos, pair_block, gate_block, key_pos
            )

        needed = jnp.logical_and(valid, first <= last_query)
        return lax.cond(needed, compute, lambda state: state, loop_state)

    return lax.fori_loop(0, piece_rows // block_rows, one_block, running)


def body(
    query_rows,
    key_rows,
    value_rows,
    pool_input,
    log_gate_sums,
    query_gain,
    key_gain,
    pool_weight,
    pool_scale,
    attention_out,
    pooling_out,
):
    length = query_rows.shape[0]
    kv_here = key_rows.shape[1] // HEAD
    ratio = QUERY_HEADS // KV_HEADS
    sp_index = lax.axis_index("sp")
    queries = head_norm(query_rows, query_gain, kv_here * ratio).reshape(
        length, kv_here, ratio, HEAD
    )
    pair = jnp.stack(
        [head_norm(key_rows, key_gain, kv_here), value_rows.reshape(length, kv_here, HEAD)]
    )
    all_gates = lax.all_gather(log_gate_sums, "sp", axis=0, tiled=True)
    query_gates = log_gate_sums.T.reshape(kv_here, ratio, length, 1)
    query_pos = sp_index * length + jnp.arange(length, dtype=jnp.int32)
    start_state = (
        jnp.full((kv_here, ratio, length, 1), masked, jnp.float32),
        jnp.zeros((kv_here, ratio, length, 1), jnp.float32),
        jnp.zeros((kv_here, ratio, length, HEAD), jnp.float32),
    )
    row_best, weight_sum, accumulated = attend_piece(
        start_state,
        lax.all_gather(pair, "sp", axis=1, tiled=True),
        queries,
        query_gates,
        query_pos,
        all_gates,
        jnp.int32(0) >= 0,
    )
    attended = (
        (accumulated / weight_sum)
        .transpose(2, 0, 1, 3)
        .reshape(length, kv_here * ratio * HEAD)
        .astype(jnp.bfloat16)
    )
    group_here = pool_input.shape[1] // GROUP
    rim = from_behind(pool_input[length - (MAX_WINDOW - 1) :], "sp", 1)
    padded = (
        jnp.concatenate([rim, pool_input])
        .astype(jnp.float32)
        .reshape(length + MAX_WINDOW - 1, group_here, GROUP)
    )
    levels = MAX_WINDOW.bit_length() - 1
    groups = lax.axis_index("tp") * group_here + jnp.arange(group_here, dtype=jnp.int32)
    windows = 2 ** (1 + groups % levels)
    pooled = window_means(padded, length, sp_index * length, windows).astype(jnp.bfloat16)
    mixing = jnp.einsum("tgc,gcd->tgd", pooled, pool_weight, preferred_element_type=jnp.float32)
    pool_mixed = (
        (mixing * pool_scale.reshape(group_here, GROUP))
        .astype(jnp.bfloat16)
        .reshape(length, group_here * GROUP)
    )
    total = jnp.dot(attended, attention_out, preferred_element_type=jnp.float32)
    return lax.psum_scatter(
        (total + jnp.dot(pool_mixed, pooling_out, preferred_element_type=jnp.float32)).astype(
            jnp.bfloat16
        ),
        "tp",
        scatter_dimension=0,
        tiled=True,
    )


def solution(mesh):
    return jax.shard_map(
        body,
        mesh=mesh,
        in_specs=(
            P(("grp", "sp"), "tp"),
            P(("grp", "sp"), "tp"),
            P(("grp", "sp"), "tp"),
            P(("grp", "sp"), "tp"),
            P(("grp", "sp"), "tp"),
            P(),
            P(),
            P("tp", None, None),
            P("tp"),
            P("tp", None),
            P("tp", None),
        ),
        out_specs=P(("grp", "sp", "tp"), None),
        check_vma=False,
    )
```

profile of v0, /device:TPU:0, one launch (start us, length us, event | category | flops | bytes accessed | tf_op | source)
XLA Modules:
  0.0 131.0 jit_solution(2364926939648079398)
XLA Ops:
  6.5 0.0 copy-start
  6.5 0.0 copy-start.3
  6.5 0.0 copy-start.5
  6.5 0.0 all-gather.2.cloned.1.call-start
  6.5 0.8 slice.110
  7.3 4.9 %collective-permute-start = (bf16[15,512]{1,0:T(8,128)(2,1)S(1)}, bf16[15,512]{1,0:T(8,128)(2,1)S(1)}, u32[]{:S(2)}, u32[]{:S(2)}) collective-permute-start(bf16[15,512]{1,0:T(8,128)(2,1)S(1)} %slice.110), channel_id=1, source_target_pairs={{0,4},{4,8},{8,12},{1,5},{5,9},{9,13},{2,6},{6,10},{10,14},{3,7},{... | collective-permute-start | bytes 46088 | tf_op jit(solution)/shard_map/ppermute | solution.py:19
  12.3 1.1 copy.32
  13.4 0.1 bitcast_reduce_fusion.1
  13.5 1.1 copy.33
  14.6 0.8 multiply_convert_fusion.1
  15.3 0.8 pad_maximum_fusion
  16.1 0.0 all-gather.2.cloned.1.call-update
  16.1 0.0 reduce-scatter.2.cloned.1.call-start
  16.2 1.2 copy.34
  17.4 0.1 bitcast_reduce_fusion
  17.6 0.1 broadcast_minimum_fusion
  17.7 0.8 multiply_convert_fusion
  18.5 0.7 mul.203
  19.2 0.6 slice.109
  19.8 0.9 copy.36
  20.7 0.0 copy-done.5
  20.7 13.7 %all_gather.7 = f32[1536,4]{0,1:T(4,128)S(1)} all-gather(f32[384,4]{0,1:T(4,128)S(1)} %copy-done.5), channel_id=1, replica_groups=mesh['grp'=2,'sp'=4,'tp'=4] {'sp'}, dimensions={0}, use_global_device_ids=true | all-gather | bytes 30720 | tf_op jit(solution)/shard_map/all_gather | solution.py:113
  34.4 0.0 collective-permute-done
  34.4 0.0 copy-done.3
  34.4 0.1 maximum_convert_fusion
  34.5 3.6 %fusion.30 = (f32[384,512]{1,0:T(8,128)S(1)}, f32[384,512]{1,0:T(8,128)S(1)}, f32[384,512]{1,0:T(8,128)S(1)}, f32[384,512]{1,0:T(8,128)S(1)}, f32[384,512]{1,0:T...) fusion(f32[399,512]{1,0:T(8,128)S(1)} %maximum_convert_fusion), kind=kLoop, calls=%fused_computation.80 | loop fusion | bytes 25165824 | tf_op jit(solution)/shard_map/slice | solution.py:33
  38.1 0.0 copy-done
  38.1 0.0 copy-start.4
  38.1 4.8 %fusion.20 = bf16[2,384,256]{1,2,0:T(8,128)(2,1)S(1)} fusion(bf16[2,256,256]{2,1,0:T(8,128)(2,1)S(1)} %copy-done, f32[2,256]{1,0:T(2,128)S(1)} %mul.203, f32[48,2,8,256]{3,2,1,0:T(8,128)S(1)} %bitcast.209, f32[48,2,8,256]{3,2,1,0:T(8,128)S(1)} %bitcast.210, f32[48,2,8,256]{3,2,1,0:T(8,128)S(1)} %bitcast.211, f32[48,2,8,256]{3,2,1,0:T(8,128)S(1)} %bitcast.212, ...), kind=kOutput, calls=%fused_computation.29 | convolution fusion | flops 105381888 | bytes 13243400 | tf_op jit(solution)/shard_map/tgc,gcd->tgd/dot_general | solution.py:147
  42.9 10.5 %all-gather.2.cloned.1.call-done = bf16[2,1536,2,128]{1,3,2,0:T(8,128)(2,1)} async-done(((bf16[2,384,2,128]{1,3,2,0:T(8,128)(2,1)}), bf16[2,1536,2,128]{1,3,2,0:T(8,128)(2,1)}) %all-gather.2.cloned.1.call-update) | async-done | bytes 1572880 | tf_op jit(solution)/shard_map/all_gather | solution.py:123
  53.3 2.6 %copy.35 = bf16[2,1536,2,128]{3,1,2,0:T(8,128)(2,1)} copy(bf16[2,1536,2,128]{1,3,2,0:T(8,128)(2,1)} %all-gather.2.cloned.1.call-done) | data formatting | bytes 3145728
  55.9 0.1 broadcast_in_dim.71
  56.0 0.0 copy-done.4
  56.0 11.9 %while.18 = (s32[]{:T(128)}, f32[2,2,384,1]{2,1,0,3:T(2,128)S(1)}, f32[2,2,384,1]{2,1,0,3:T(2,128)S(1)}, f32[2,2,384,128]{3,2,1,0:T(8,128)S(1)}, s32[]{:T(128)},...) while((s32[]{:T(128)}, f32[2,2,384,1]{2,1,0,3:T(2,128)S(1)}, ...), condition=%wide.region_7.8_spmd.clone, body=%wide.region_2.7_spmd.clone.sunk | while | flops 627086976 | bytes 37177752 | solution.py:87
  56.6 10.6 %conditional.3 = ((f32[2,2,384,1]{2,1,0,3:T(2,128)S(1)}, f32[2,2,384,1]{2,1,0,3:T(2,128)S(1)}, f32[2,2,384,128]{3,2,1,0:T(8,128)S(1)})) conditional(s32[]{:T(128)} %convert_element_type.104, (f32[2,2,384,1]{2,1,0,3:T(2,128)S(1)}, f32[2,2,384,1]{2,1,0,3:T(2,128)S(1)}, f32[2,2,384,128]{3,2,1,0:T(8,128)S(1)}) %tuple.62, (s32[]{:T(128)}, s32[]{:T(128)}, ...), branch_computations={%region_3.0_spmd, %region_4.6_spmd} | conditional | flops 627086976 | bytes 37175960 | solution.py:85
  56.7 0.2 broadcast_compare_fusion
  56.9 0.1 dynamic-slice_bitcast_fusion.4
  57.0 3.9 %fusion.6 = (f32[2,2,384]{2,1,0:T(2,128)S(1)}, f32[2,768,384,2]{2,1,3,0:T(8,128)}) fusion(f32[2,2,768]{2,1,0:T(2,128)S(1)} %sub.6, f32[2,2,384]{2,1,0:T(2,128)S(1)} %bitcast.231, pred[384,768]{0,1:T(8,128)(4,1)S(1)} %broadcast_compare_fusion, bf16[384,2,2,128]{3,0,2,1:T(8,128)(2,1)S(1)} %get-tuple-element.199, ...), kind=kOutput, calls=%fused_computation.7 | convolution fusion | flops 307886592 | bytes 5824516 | tf_op jit(solution)/shard_map/while/body/eval_jaxpr/cond/branch_1_fun/tkrd,skd->krts/dot_general | solution.py:44
  60.9 0.0 copy-start.1
  61.0 4.6 %fusion.10 = f32[2,2,384,128]{3,2,1,0:T(8,128)S(1)} fusion(f32[2,768,384,2]{2,1,3,0:T(8,128)} %get-tuple-element.284, f32[2,2,384]{2,1,0:T(2,128)S(1)} %bitcast.224, f32[2,2,768]{2,1,0:T(2,128)S(1)} %sub.6, f32[2,2,384]{2,1,0:T(2,128)S(1)} %bitcast.232, pred[384,768]{0,1:T(8,128)(4,1)S(1)} %broadcast_compare_fusion, ...), kind=kOutput, calls=%fused_computation.10 | convolution fusion | flops 310640640 | bytes 7010312 | tf_op jit(solution)/shard_map/while/body/eval_jaxpr/cond/branch_1_fun/krts,skd->krtd/dot_general | solution.py:54
  65.6 0.0 copy-done.1
  65.6 1.6 %fusion.5 = f32[2,2,384]{2,1,0:T(2,128)S(1)} fusion(f32[2,768,384,2]{2,1,3,0:T(8,128)S(1)} %copy-done.1, f32[2,2,384]{2,1,0:T(2,128)S(1)} %bitcast.225, f32[2,2,768]{2,1,0:T(2,128)S(1)} %sub.6, f32[2,2,384]{2,1,0:T(2,128)S(1)} %bitcast.233, pred[384,768]{0,1:T(8,128)(4,1)S(1)} %broadcast_compare_fusion), kind=kLoop, calls=%fused_computation.6 | loop fusion | flops 8256000 | bytes 5044224 | tf_op jit(solution)/shard_map/while/body/eval_jaxpr/cond/branch_1_fun/reduce_sum | solution.py:53
  67.9 0.3 copy.37
  68.2 0.1 divide_convert_fusion
  68.2 0.0 copy-start.2
  68.2 4.2 %fusion.31 = f32[384,4096]{1,0:T(8,128)S(1)} fusion(bf16[384,512]{0,1:T(8,128)(2,1)S(1)} %bitcast.228, bf16[512,4096]{1,0:T(8,128)(2,1)} %param.24), kind=kOutput, calls=%fused_computation.81 | convolution fusion | flops 1610612736 | bytes 10878976 | tf_op jit(solution)/shard_map/dot_general | solution.py:153
  72.5 0.0 copy-done.2
  72.5 3.7 %add_convert_fusion = bf16[384,4096]{1,0:T(8,128)(2,1)} fusion(f32[384,4096]{1,0:T(8,128)S(1)} %fusion.31, bf16[384,512]{0,1:T(8,128)(2,1)S(1)} %bitcast.227, bf16[512,4096]{1,0:T(8,128)(2,1)S(1)} %copy-done.2), kind=kOutput, calls=%fused_computation.27 | convolution fusion | flops 1613758464 | bytes 14024704 | tf_op jit(solution)/shard_map/dot_general | solution.py:155
  76.2 0.0 reduce-scatter.2.cloned.1.call-update
  76.2 48.0 %reduce-scatter.2.cloned.1.call-done = bf16[96,4096]{1,0:T(8,128)(2,1)} async-done(((bf16[384,4096]{1,0:T(8,128)(2,1)}), bf16[96,4096]{1,0:T(8,128)(2,1)}) %reduce-scatter.2.cloned.1.call-update) | async-done | bytes 786448 | tf_op jit(solution)/shard_map/reduce_scatter | solution.py:154
  (20 shorter events, 0.2 us)
Async XLA Ops:
  6.5 31.6 %copy-start = (bf16[2,256,256]{2,1,0:T(8,128)(2,1)S(1)}, bf16[2,256,256]{2,1,0:T(8,128)(2,1)}, u32[]{:S(2)}) copy-start(bf16[2,256,256]{2,1,0:T(8,128)(2,1)} %param.22) | copy-start | bytes 786436
  6.5 27.9 %copy-start.3 = (bf16[384,512]{1,0:T(8,128)(2,1)S(1)}, bf16[384,512]{1,0:T(8,128)(2,1)}, u32[]{:S(2)}) copy-start(bf16[384,512]{1,0:T(8,128)(2,1)} %param.18) | copy-start | bytes 1179652
  6.5 14.2 %copy-start.5 = (f32[384,4]{0,1:T(4,128)S(1)}, f32[384,4]{0,1:T(4,128)}, u32[]{:S(2)}) copy-start(f32[384,4]{0,1:T(4,128)} %param.19) | copy-start | bytes 18436
  6.5 46.8 %all-gather.2.cloned.1.call-start = ((), (), s32[]{:S(2)}) async-start(), calls=%async_computation.1 | async-start | bytes 1966080 | tf_op jit(solution)/shard_map/all_gather | solution.py:123
  7.3 27.1 %collective-permute-start = (bf16[15,512]{1,0:T(8,128)(2,1)S(1)}, bf16[15,512]{1,0:T(8,128)(2,1)S(1)}, u32[]{:S(2)}, u32[]{:S(2)}) collective-permute-start(bf16[15,512]{1,0:T(8,128)(2,1)S(1)} %slice.110), channel_id=1, source_target_pairs={{0,4},{4,8},{8,12},{1,5},{5,9},{9,13},{2,6},{6,10},{10,14},{3,7},{... | collective-permute-start | bytes 46088 | tf_op jit(solution)/shard_map/ppermute | solution.py:19
  16.1 108.1 %reduce-scatter.2.cloned.1.call-start = ((), (), s32[]{:S(2)}) async-start(), calls=%async_computation.2 | async-start | bytes 3932160 | tf_op jit(solution)/shard_map/reduce_scatter | solution.py:154
  38.1 17.9 %copy-start.4 = (bf16[384,2,2,128]{3,0,2,1:T(8,128)(2,1)S(1)}, bf16[384,2,2,128]{3,0,2,1:T(8,128)(2,1)}, u32[]{:S(2)}) copy-start(bf16[384,2,2,128]{3,0,2,1:T(8,128)(2,1)} %copy.36) | copy-start | bytes 1179652
  60.9 4.6 %copy-start.1 = (f32[2,768,384,2]{2,1,3,0:T(8,128)S(1)}, f32[2,768,384,2]{2,1,3,0:T(8,128)}, u32[]{:S(2)}) copy-start(f32[2,768,384,2]{2,1,3,0:T(8,128)} %get-tuple-element.284) | copy-start | bytes 14155780 | tf_op jit(solution)/shard_map/while/body/eval_jaxpr/cond
  68.2 4.3 %copy-start.2 = (bf16[512,4096]{1,0:T(8,128)(2,1)S(1)}, bf16[512,4096]{1,0:T(8,128)(2,1)}, u32[]{:S(2)}) copy-start(bf16[512,4096]{1,0:T(8,128)(2,1)} %param.25) | copy-start | bytes 12582916
Sparse Core Ops, SparseCore 0:
  16.3 37.0 all-gather.1
  76.3 47.8 reduce-scatter.1
where the time goes:
time: 131 us
  waiting for transfers between devices  58.5 us (45%)
  matrix products  21.2 us (16%)
  blocking collectives  13.7 us (10%)
  between operations  13.6 us (10%)
  local copies, waits for them, and re-layouts  13 us (10%)
  starting transfers between devices  4.99 us (4%)
  other arithmetic  4.75 us (4%)
  loops' own time  1.31 us (1%)
    reduce_scatter x1, waiting for transfers between devices, body(): lax.psum_scatter((total + jnp.dot(pool_mixed, pooling_out, preferred_elem...  48 us
    all_gather x1, blocking collectives, body(): all_gates = lax.all_gather(log_gate_sums, 'sp', axis=0, tiled=True)  13.7 us
    all_gather x1, waiting for transfers between devices, body(): lax.all_gather(pair, 'sp', axis=1, tiled=True)  10.5 us
    unnamed x15, local copies, waits for them, and re-layouts  6.93 us
    ppermute x1, starting transfers between devices, from_behind(): return lax.ppermute(block, axis, route)  4.94 us
    dot_general x1, matrix products, body(): jnp.einsum('tgc,gcd->tgd', pooled, pool_weight, preferred_element_type=jn...  4.77 us
    dot_general x1, matrix products, attend_block(): jnp.einsum('krts,skd->krtd', weights.astype(jnp.bfloat16), pair_block[1],...  4.59 us
    dot_general x1, matrix products, body(): total = jnp.dot(attended, attention_out, preferred_element_type=jnp.float32)  4.24 us
  transfers between devices with their start and end apart: 3, of which 2 were waited for; matrix products, arithmetic and copies ran while one was open for 13% of the time, Pallas kernels for 0%

commit v1 on v0

--- a/solution.py
+++ b/solution.py
@@ -120,7 +120,9 @@
     )
     row_best, weight_sum, accumulated = attend_piece(
         start_state,
-        lax.all_gather(pair, "sp", axis=1, tiled=True),
+        jnp.concatenate(
+            lax.all_to_all(jnp.stack([pair] * lax.axis_size("sp")), "sp", 0, 0), axis=1
+        ),
         queries,
         query_gates,
         query_pos,

time: 131 us -> 153 us (1.17)
  blocking collectives: 13.7 us -> 39.9 us
  waiting for transfers between devices: 58.5 us -> 48.9 us
  starting transfers between devices: 4.99 us -> 8.81 us
    all_gather x1, blocking collectives: 13.7 us -> 39.9 us  [body(): all_gates = lax.all_gather(log_gate_sums, 'sp', axis=0, tiled=True)]
    all_gather x1 -> x0, waiting for transfers between devices: 10.5 us -> none  [body(): lax.all_gather(pair, 'sp', axis=1, tiled=True)]
    unnamed x15 -> x16, local copies, waits for them, and re-layouts: 6.93 us -> 1.19 us
    all_to_all x0 -> x1, starting transfers between devices: none -> 3.86 us  [body(): lax.all_to_all(jnp.stack([pair] * lax.axis_size('sp')), 'sp', 0, 0)]
    another operation x0 -> x3, local copies, waits for them, and re-layouts: none -> 2.48 us  [the longest x1 1.46 us: body(): jnp.stack([pair] * lax.axis_size('sp'))]
  transfers between devices with their start and end apart: 3 -> 3, of which waited for: 2 -> 1; matrix products, arithmetic and copies ran while one was open for 13% -> 12% of each run, Pallas kernels for 0% -> 0%
where the time goes in v1:
time: 153 us; the launch traced here: 152 us
  waiting for transfers between devices  48.9 us (32%)
  blocking collectives  39.9 us (26%)
  matrix products  21.6 us (14%)
  between operations  13.7 us (9%)
  local copies, waits for them, and re-layouts  12.2 us (8%)
  starting transfers between devices  8.81 us (6%)
  other arithmetic  5.78 us (4%)
    reduce_scatter x1, waiting for transfers between devices, body(): lax.psum_scatter((total + jnp.dot(pool_mixed, pooling_out, preferred_elem...  48.9 us
    all_gather x1, blocking collectives, body(): all_gates = lax.all_gather(log_gate_sums, 'sp', axis=0, tiled=True)  39.9 us
    dot_general x1, matrix products, body(): jnp.einsum('tgc,gcd->tgd', pooled, pool_weight, preferred_element_type=jn...  5.09 us
    ppermute x1, starting transfers between devices, from_behind(): return lax.ppermute(block, axis, route)  4.94 us
    dot_general x1, matrix products, attend_block(): jnp.einsum('krts,skd->krtd', weights.astype(jnp.bfloat16), pair_block[1],...  4.6 us
    dot_general x1, matrix products, body(): total = jnp.dot(attended, attention_out, preferred_element_type=jnp.float32)  4.23 us
    slice x1, local copies, waits for them, and re-layouts, window_means(): padded[rim_rows - lookback:rim_rows - lookback + length]  3.98 us
    dot_general x1, matrix products, attend_block(): jnp.einsum('tkrd,skd->krts', queries, pair_block[0], preferred_element_ty...  3.96 us
  transfers between devices with their start and end apart: 3, of which 1 were waited for; matrix products, arithmetic and copies ran while one was open for 12% of the time, Pallas kernels for 0%

profile of v1, /device:TPU:0, one launch (start us, length us, event | category | flops | bytes accessed | tf_op | source)
XLA Modules:
  0.0 152.3 jit_solution(9594187118769713685)
XLA Ops:
  6.5 0.0 copy-start
  6.5 0.8 slice.110
  7.3 4.9 %collective-permute-start = (bf16[15,512]{1,0:T(8,128)(2,1)S(1)}, bf16[15,512]{1,0:T(8,128)(2,1)S(1)}, u32[]{:S(2)}, u32[]{:S(2)}) collective-permute-start(bf16[15,512]{1,0:T(8,128)(2,1)S(1)} %slice.110), channel_id=1, source_target_pairs={{0,4},{4,8},{8,12},{1,5},{5,9},{9,13},{2,6},{6,10},{10,14},{3,7},{... | collective-permute-start | bytes 46088 | tf_op jit(solution)/shard_map/ppermute | solution.py:19
  12.3 1.0 convert_multiply_fusion.1
  13.2 0.0 copy-start.3
  13.2 1.2 reshape.188
  14.4 0.2 mul.187
  14.6 0.0 copy-start.7
  14.6 0.5 reduce_sum.27
  15.1 0.0 copy-start.6
  15.1 0.1 copy.131
  15.2 1.0 stack_reshape.3
  16.3 0.0 copy-start.5
  16.3 0.8 fusion.26
  17.2 1.5 stack.5
  18.6 3.9 %all-to-all-start = ((bf16[4,2,384,2,128]{4,2,3,1,0:T(8,128)(2,1)}), bf16[4,2,384,2,128]{4,2,3,1,0:T(8,128)(2,1)S(1)}, u32[]{:S(2)}, u32[]{:S(2)}) async-start(bf16[4,2,384,2,128]{4,2,3,1,0:T(8,128)(2,1)} %stack.5), calls=%async_computation | async-start | bytes 3145728 | tf_op jit(solution)/shard_map/all_to_all | solution.py:124
  22.5 0.0 reduce-scatter.2.cloned.1.call-start
  22.5 0.0 copy-done.3
  22.5 0.2 copy.135
  22.7 0.1 bitcast_reduce_fusion
  22.9 0.1 broadcast_minimum_fusion
  23.0 0.0 copy-done.7
  23.0 0.1 multiply_convert_fusion
  23.1 0.0 copy-done.6
  23.2 0.6 slice.109
  23.8 0.9 copy.136
  24.7 0.0 copy-done.5
  24.7 39.9 %all_gather.3 = f32[1536,4]{0,1:T(4,128)S(1)} all-gather(f32[384,4]{0,1:T(4,128)S(1)} %copy-done.5), channel_id=1, replica_groups=mesh['grp'=2,'sp'=4,'tp'=4] {'sp'}, dimensions={0}, use_global_device_ids=true | all-gather | bytes 30720 | tf_op jit(solution)/shard_map/all_gather | solution.py:113
  64.6 0.0 collective-permute-done
  64.6 1.1 maximum_convert_fusion
  65.7 4.0 %fusion.32 = (f32[384,512]{1,0:T(8,128)S(1)}, f32[384,512]{1,0:T(8,128)S(1)}, f32[384,512]{1,0:T(8,128)S(1)}, f32[384,512]{1,0:T(8,128)}, f32[384,512]{1,0:T(8,1...) fusion(f32[399,512]{1,0:T(8,128)S(1)} %maximum_convert_fusion), kind=kLoop, calls=%fused_computation.81 | loop fusion | bytes 25165824 | tf_op jit(solution)/shard_map/slice | solution.py:33
  69.7 0.0 copy-done
  69.7 0.0 copy-start.4
  69.7 5.1 %fusion.20 = bf16[2,384,256]{1,2,0:T(8,128)(2,1)S(1)} fusion(bf16[2,256,256]{2,1,0:T(8,128)(2,1)S(1)} %copy-done, f32[2,256]{1,0:T(2,128)S(1)} %mul.203, f32[48,2,8,256]{3,2,1,0:T(8,128)S(1)} %bitcast.207, f32[48,2,8,256]{3,2,1,0:T(8,128)S(1)} %bitcast.208, f32[48,2,8,256]{3,2,1,0:T(8,128)} %bitcast.209, f32[48,2,8,256]{3,2,1,0:T(8,128)} %bitcast.210, ...), kind=kOutput, calls=%fused_computation.29 | convolution fusion | flops 105381888 | bytes 13243400 | tf_op jit(solution)/shard_map/tgc,gcd->tgd/dot_general | solution.py:149
  74.8 0.0 all-to-all-done
  74.8 1.3 copy.134
  76.1 0.1 broadcast_in_dim.71
  76.2 0.0 copy-done.4
  76.2 12.0 %while.18 = (s32[]{:T(128)}, f32[2,2,384,1]{2,1,0,3:T(2,128)S(1)}, f32[2,2,384,1]{2,1,0,3:T(2,128)S(1)}, f32[2,2,384,128]{3,2,1,0:T(8,128)S(1)}, s32[]{:T(128)},...) while((s32[]{:T(128)}, f32[2,2,384,1]{2,1,0,3:T(2,128)S(1)}, ...), condition=%wide.region_7.8_spmd.clone, body=%wide.region_2.7_spmd.clone.sunk | while | flops 627086976 | bytes 37177752 | solution.py:87
  76.8 10.7 %conditional.3 = ((f32[2,2,384,1]{2,1,0,3:T(2,128)S(1)}, f32[2,2,384,1]{2,1,0,3:T(2,128)S(1)}, f32[2,2,384,128]{3,2,1,0:T(8,128)S(1)})) conditional(s32[]{:T(128)} %convert_element_type.102, (f32[2,2,384,1]{2,1,0,3:T(2,128)S(1)}, f32[2,2,384,1]{2,1,0,3:T(2,128)S(1)}, f32[2,2,384,128]{3,2,1,0:T(8,128)S(1)}) %tuple.66, (s32[]{:T(128)}, s32[]{:T(128)}, ...), branch_computations={%region_3.0_spmd, %region_4.6_spmd} | conditional | flops 627086976 | bytes 37175960 | solution.py:85
  76.9 0.2 broadcast_compare_fusion
  77.1 0.1 dynamic-slice_bitcast_fusion.4
  77.2 4.0 %fusion.6 = (f32[2,2,384]{2,1,0:T(2,128)S(1)}, f32[2,768,384,2]{2,1,3,0:T(8,128)}) fusion(f32[2,2,768]{2,1,0:T(2,128)S(1)} %sub.6, f32[2,2,384]{2,1,0:T(2,128)S(1)} %bitcast.228, pred[384,768]{0,1:T(8,128)(4,1)S(1)} %broadcast_compare_fusion, bf16[384,2,2,128]{3,0,2,1:T(8,128)(2,1)S(1)} %get-tuple-element.199, ...), kind=kOutput, calls=%fused_computation.7 | convolution fusion | flops 307886592 | bytes 5824516 | tf_op jit(solution)/shard_map/while/body/eval_jaxpr/cond/branch_1_fun/tkrd,skd->krts/dot_general | solution.py:44
  81.2 0.0 copy-start.1
  81.2 4.6 %fusion.10 = f32[2,2,384,128]{3,2,1,0:T(8,128)S(1)} fusion(f32[2,768,384,2]{2,1,3,0:T(8,128)} %get-tuple-element.324, f32[2,2,384]{2,1,0:T(2,128)S(1)} %bitcast.222, f32[2,2,768]{2,1,0:T(2,128)S(1)} %sub.6, f32[2,2,384]{2,1,0:T(2,128)S(1)} %bitcast.229, pred[384,768]{0,1:T(8,128)(4,1)S(1)} %broadcast_compare_fusion, ...), kind=kOutput, calls=%fused_computation.10 | convolution fusion | flops 310640640 | bytes 7010312 | tf_op jit(solution)/shard_map/while/body/eval_jaxpr/cond/branch_1_fun/krts,skd->krtd/dot_general | solution.py:54
  85.8 0.0 copy-done.1
  85.8 1.7 %fusion.5 = f32[2,2,384]{2,1,0:T(2,128)S(1)} fusion(f32[2,768,384,2]{2,1,3,0:T(8,128)S(1)} %copy-done.1, f32[2,2,384]{2,1,0:T(2,128)S(1)} %bitcast.223, f32[2,2,768]{2,1,0:T(2,128)S(1)} %sub.6, f32[2,2,384]{2,1,0:T(2,128)S(1)} %bitcast.230, pred[384,768]{0,1:T(8,128)(4,1)S(1)} %broadcast_compare_fusion), kind=kLoop, calls=%fused_computation.6 | loop fusion | flops 8256000 | bytes 5044224 | tf_op jit(solution)/shard_map/while/body/eval_jaxpr/cond/branch_1_fun/reduce_sum | solution.py:53
  88.2 0.3 copy.137
  88.5 0.1 divide_convert_fusion
  88.6 0.0 copy-start.2
  88.6 4.2 %fusion.33 = f32[384,4096]{1,0:T(8,128)S(1)} fusion(bf16[384,512]{0,1:T(8,128)(2,1)S(1)} %bitcast.226, bf16[512,4096]{1,0:T(8,128)(2,1)} %param.24), kind=kOutput, calls=%fused_computation.82 | convolution fusion | flops 1610612736 | bytes 10878976 | tf_op jit(solution)/shard_map/dot_general | solution.py:155
  92.8 0.0 copy-done.2
  92.8 3.7 %add_convert_fusion = bf16[384,4096]{1,0:T(8,128)(2,1)} fusion(f32[384,4096]{1,0:T(8,128)S(1)} %fusion.33, bf16[384,512]{0,1:T(8,128)(2,1)S(1)} %bitcast.224, bf16[512,4096]{1,0:T(8,128)(2,1)S(1)} %copy-done.2), kind=kOutput, calls=%fused_computation.27 | convolution fusion | flops 1613758464 | bytes 14024704 | tf_op jit(solution)/shard_map/dot_general | solution.py:157
  96.5 0.0 reduce-scatter.2.cloned.1.call-update
  96.5 48.9 %reduce-scatter.2.cloned.1.call-done = bf16[96,4096]{1,0:T(8,128)(2,1)} async-done(((bf16[384,4096]{1,0:T(8,128)(2,1)}), bf16[96,4096]{1,0:T(8,128)(2,1)}) %reduce-scatter.2.cloned.1.call-update) | async-done | bytes 786448 | tf_op jit(solution)/shard_map/reduce_scatter | solution.py:156
  (23 shorter events, 0.3 us)
Async XLA Ops:
  6.5 63.2 %copy-start = (bf16[2,256,256]{2,1,0:T(8,128)(2,1)S(1)}, bf16[2,256,256]{2,1,0:T(8,128)(2,1)}, u32[]{:S(2)}) copy-start(bf16[2,256,256]{2,1,0:T(8,128)(2,1)} %param.22) | copy-start | bytes 786436
  7.3 57.3 %collective-permute-start = (bf16[15,512]{1,0:T(8,128)(2,1)S(1)}, bf16[15,512]{1,0:T(8,128)(2,1)S(1)}, u32[]{:S(2)}, u32[]{:S(2)}) collective-permute-start(bf16[15,512]{1,0:T(8,128)(2,1)S(1)} %slice.110), channel_id=1, source_target_pairs={{0,4},{4,8},{8,12},{1,5},{5,9},{9,13},{2,6},{6,10},{10,14},{3,7},{... | collective-permute-start | bytes 46088 | tf_op jit(solution)/shard_map/ppermute | solution.py:19
  13.2 9.3 %copy-start.3 = (bf16[384,512]{1,0:T(8,128)(2,1)S(1)}, bf16[384,512]{1,0:T(8,128)(2,1)}, u32[]{:S(2)}) copy-start(bf16[384,512]{1,0:T(8,128)(2,1)} %param.15) | copy-start | bytes 1179652
  14.6 8.4 %copy-start.7 = (f32[128]{0:T(128)S(1)}, f32[128]{0:T(128)}, u32[]{:S(2)}) copy-start(f32[128]{0:T(128)} %param.20) | copy-start | bytes 1540
  15.1 8.0 %copy-start.6 = (f32[512]{0:T(512)S(1)}, f32[512]{0:T(512)}, u32[]{:S(2)}) copy-start(f32[512]{0:T(512)} %param.23) | copy-start | bytes 6148
  16.3 8.5 %copy-start.5 = (f32[384,4]{0,1:T(4,128)S(1)}, f32[384,4]{0,1:T(4,128)}, u32[]{:S(2)}) copy-start(f32[384,4]{0,1:T(4,128)} %param.19) | copy-start | bytes 18436
  18.6 56.2 %all-to-all-start = ((bf16[4,2,384,2,128]{4,2,3,1,0:T(8,128)(2,1)}), bf16[4,2,384,2,128]{4,2,3,1,0:T(8,128)(2,1)S(1)}, u32[]{:S(2)}, u32[]{:S(2)}) async-start(bf16[4,2,384,2,128]{4,2,3,1,0:T(8,128)(2,1)} %stack.5), calls=%async_computation | async-start | bytes 3145728 | tf_op jit(solution)/shard_map/all_to_all | solution.py:124
  22.5 123.0 %reduce-scatter.2.cloned.1.call-start = ((), (), s32[]{:S(2)}) async-start(), calls=%async_computation.2 | async-start | bytes 3932160 | tf_op jit(solution)/shard_map/reduce_scatter | solution.py:156
  69.7 6.5 %copy-start.4 = (bf16[384,2,2,128]{3,0,2,1:T(8,128)(2,1)S(1)}, bf16[384,2,2,128]{3,0,2,1:T(8,128)(2,1)}, u32[]{:S(2)}) copy-start(bf16[384,2,2,128]{3,0,2,1:T(8,128)(2,1)} %copy.136) | copy-start | bytes 1179652
  81.2 4.6 %copy-start.1 = (f32[2,768,384,2]{2,1,3,0:T(8,128)S(1)}, f32[2,768,384,2]{2,1,3,0:T(8,128)}, u32[]{:S(2)}) copy-start(f32[2,768,384,2]{2,1,3,0:T(8,128)} %get-tuple-element.324) | copy-start | bytes 14155780 | tf_op jit(solution)/shard_map/while/body/eval_jaxpr/cond
  88.6 4.2 %copy-start.2 = (bf16[512,4096]{1,0:T(8,128)(2,1)S(1)}, bf16[512,4096]{1,0:T(8,128)(2,1)}, u32[]{:S(2)}) copy-start(bf16[512,4096]{1,0:T(8,128)(2,1)} %param.25) | copy-start | bytes 12582916
Sparse Core Ops, SparseCore 0:
  96.7 48.7 reduce-scatter.1
